TPU v7x, 128 devices: a whole 4x4x4 slice. The times are simulated.
128 devices in a mesh: rep: 2 (over z_hi), fs: 32 (over z_lo, y, x), tp: 2 (over core).
Axes of the slice: x: 4, y: 4, z: 4 (z_hi: 2, z_lo: 2; z = z_hi * 2 + z_lo), core: 2. Of those that a mesh axis runs over, the one named last changes fastest.
Arguments:
- sequence: bfloat16 [64, 768, 2048], P(('rep', 'fs'), None, 'tp'), may hold values from -6 to 6
- mix_gain: float32 [2048], replicated, may hold values from 0.1 to 1.9
- ffn_gain: float32 [2048], replicated, may hold values from 0.1 to 1.9
- proj_outer: float32 [2048, 2048], P(None, ('tp', 'fs')), may hold values from -0.125 to 0.125
- proj_inner: float32 [2048, 2048], P(None, ('tp', 'fs')), may hold values from -0.125 to 0.125
- proj_value: float32 [2048, 2048], P(None, ('tp', 'fs')), may hold values from -0.125 to 0.125
- proj_scales: float32 [3, 2048], P(None, 'tp'), may hold values from 0.5 to 2
- taps: float32 [3, 2048], P(None, 'tp'), may hold values from -3 to 3
- mix_out: float32 [2048, 2048], P('tp', 'fs'), may hold values from -0.125 to 0.125
- mix_out_scale: float32 [2048], P('fs'), may hold values from 0.5 to 2
- ffn_gate: float32 [2048, 2816], P(None, ('tp', 'fs')), may hold values from -0.125 to 0.125
- ffn_up: float32 [2048, 2816], P(None, ('tp', 'fs')), may hold values from -0.125 to 0.125
- ffn_scales: float32 [2, 2816], P(None, 'tp'), may hold values from 0.5 to 2
- ffn_down: float32 [2816, 2048], P('tp', 'fs'), may hold values from -0.109375 to 0.109375
- down_scale: float32 [2048], P('fs'), may hold values from 0.5 to 2
Outputs:
- layer_out: bfloat16 [64, 768, 2048], P(('rep', 'fs'), None, 'tp')
All inputs are finite; a program needn't handle non-finite values.
Results may differ from a plain program's by a relative error of at most 0.013.
Values may be sent and summed in bfloat16 or wider, within the bound.
A program may use at most 128 MiB of HBM per device.

v0:
```python
import jax
import jax.numpy as jnp
from jax import lax
from jax.sharding import PartitionSpec as P

eps = 1e-06


def gather_turned(arrays, axis, dims):
    turned = [jnp.moveaxis(a, dim, 0) for a, dim in zip(arrays, dims)]
    both = jnp.concatenate([t.reshape(len(t), -1) for t in turned], axis=1)
    out, at, outs = (lax.all_gather(both, axis, axis=0, tiled=True), 0, [])
    for t, dim in zip(turned, dims):
        share = out[:, at : at + t[0].size].reshape(-1, *t.shape[1:])
        outs.append(jnp.moveaxis(share, 0, dim))
        at += t[0].size
    return tuple(outs)


def in_blocks(array, dim, devices):
    lengths = array.shape
    blocks = array.reshape(*lengths[:dim], devices, lengths[dim] // devices, *lengths[dim + 1 :])
    return jnp.moveaxis(blocks, dim, 0)


def sent_and_summed(array, axis, dim):
    blocks = in_blocks(array, dim, lax.axis_size(axis))
    arrived = lax.all_to_all(blocks, axis, split_axis=0, concat_axis=0, tiled=True)
    return arrived.astype(jnp.float32).sum(axis=0)


def rms_rows(rows, gain):
    values = rows.astype(jnp.float32)
    scaled = values * lax.rsqrt(jnp.mean(values * values, axis=-1, keepdims=True) + eps)
    return (scaled * gain).astype(jnp.bfloat16)


def body(
    sequence,
    mix_gain,
    ffn_gain,
    proj_outer,
    proj_inner,
    proj_value,
    proj_scales,
    taps,
    mix_out,
    mix_out_scale,
    ffn_gate,
    ffn_up,
    ffn_scales,
    ffn_down,
    down_scale,
):
    local = sequence[0]
    full_rows = lax.all_gather(local, "tp", axis=1, tiled=True)
    normed = rms_rows(full_rows, mix_gain)
    out_scales = gather_turned((mix_out_scale, down_scale), "fs", (0, 0))
    w_outer = proj_outer.astype(jnp.bfloat16)
    w_inner = proj_inner.astype(jnp.bfloat16)
    w_value = proj_value.astype(jnp.bfloat16)
    whole_outer, whole_inner, whole_value = gather_turned(
        (w_outer, w_inner, w_value), "fs", (1, 1, 1)
    )
    outer = jnp.dot(normed, whole_outer, preferred_element_type=jnp.float32)
    inner = jnp.dot(normed, whole_inner, preferred_element_type=jnp.float32)
    value = jnp.dot(normed, whole_value, preferred_element_type=jnp.float32)
    carried = inner * proj_scales[1] * (value * proj_scales[2])
    length = carried.shape[0]
    back_one = jnp.pad(carried, ((1, 0), (0, 0)))[:length]
    back_two = jnp.pad(carried, ((2, 0), (0, 0)))[:length]
    conv = taps[0] * back_two + taps[1] * back_one + taps[2] * carried
    gated = (outer * proj_scales[0] * conv).astype(jnp.bfloat16)
    scale = out_scales[0]
    mixer_terms = (
        jnp.dot(
            gated,
            lax.all_gather(mix_out.astype(jnp.bfloat16), "fs", axis=1, tiled=True),
            preferred_element_type=jnp.float32,
        )
        * scale
    )
    mix = sent_and_summed(mixer_terms.astype(jnp.bfloat16), "tp", 1)
    after = (local.astype(jnp.float32) + mix).astype(jnp.bfloat16)
    after_rows = lax.all_gather(after, "tp", axis=1, tiled=True)
    normed2 = rms_rows(after_rows, ffn_gain)
    w_gate = ffn_gate.astype(jnp.bfloat16)
    w_up = ffn_up.astype(jnp.bfloat16)
    whole_gate, whole_up = gather_turned((w_gate, w_up), "fs", (1, 1))
    gate = jnp.dot(normed2, whole_gate, preferred_element_type=jnp.float32)
    up = jnp.dot(normed2, whole_up, preferred_element_type=jnp.float32)
    hidden = (jax.nn.silu(gate * ffn_scales[0]) * (up * ffn_scales[1])).astype(jnp.bfloat16)
    scale = out_scales[1]
    ffn_terms = (
        jnp.dot(
            hidden,
            lax.all_gather(ffn_down.astype(jnp.bfloat16), "fs", axis=1, tiled=True),
            preferred_element_type=jnp.float32,
        )
        * scale
    )
    ffn = sent_and_summed(ffn_terms.astype(jnp.bfloat16), "tp", 1)
    result = (after.astype(jnp.float32) + ffn).astype(jnp.bfloat16)
    return result[None]


def solution(mesh):
    in_specs = (
        P(("rep", "fs"), None, "tp"),
        P(),
        P(),
        P(None, ("tp", "fs")),
        P(None, ("tp", "fs")),
        P(None, ("tp", "fs")),
        P(None, "tp"),
        P(None, "tp"),
        P("tp", "fs"),
        P("fs"),
        P(None, ("tp", "fs")),
        P(None, ("tp", "fs")),
        P(None, "tp"),
        P("tp", "fs"),
        P("fs"),
    )
    out_specs = P(("rep", "fs"), None, "tp")
    return jax.shard_map(body, mesh=mesh, in_specs=in_specs, out_specs=out_specs, check_vma=False)
```

profile of v0, /device:TPU:1, one launch (start us, length us, event | category | flops | bytes accessed | tf_op | source)
XLA Modules:
  0.0 752.1 jit_solution(7647889185761469245)
XLA Ops:
  6.5 0.0 copy-start.6
  6.5 0.0 copy-start.4
  6.5 0.0 copy-start.3
  6.5 0.0 copy-start.8
  6.6 0.0 copy-start.9
  6.6 0.0 all-gather.18.cloned.1.call-start
  6.6 0.7 all-gather.18.cloned.1.call-update
  7.3 0.0 all-gather.10.cloned.1.call-start
  7.3 1.0 convert_bitcast_fusion.5
  8.3 1.1 convert_bitcast_fusion.3
  9.4 0.8 pad_maximum_fusion
  10.2 0.0 all-gather.10.cloned.1.call-update
  10.2 0.0 copy-start.12
  10.2 0.0 all-gather.12.cloned.1.call-start
  10.2 0.0 copy-done.6
  10.3 0.7 convert_element_type.82
  10.9 0.0 all-gather.12.cloned.1.call-update
  10.9 0.0 all-gather.20.cloned.1.call-start
  11.0 0.0 copy-done.4
  11.0 0.0 copy-done.3
  11.1 0.8 maximum_bitcast_fusion
  11.9 0.0 all-gather.20.cloned.1.call-update
  11.9 0.0 all-gather.14.cloned.1.call-start
  11.9 0.0 copy-done.11
  12.0 0.0 copy-done.10
  12.0 72.3 %all-gather.1 = f32[32,64,2]{1,2,0:T(2,128)S(1)} all-gather(f32[1,64,2]{1,2,0:T(2,128)S(1)} %maximum_bitcast_fusion.1), channel_id=1, replica_groups=mesh['rep'=2,'fs'=32,'tp'=2] {'fs'}, dimensions={0}, use_global_device_ids=true | all-gather | bytes 16896 | tf_op jit(solution)/shard_map/all_gather | solution.py:12
  84.3 0.1 reshape.42
  84.4 0.0 copy-done.8
  84.4 0.0 copy-done.9
  84.5 0.0 all-gather.18.cloned.1.call-done
  84.5 2.6 fusion.3
  87.1 0.0 copy-start.2
  87.1 100.5 %all-gather.10.cloned.1.call-done = bf16[1024,6144]{1,0:T(8,128)(2,1)} async-done(((bf16[32,6144]{1,0:T(8,128)(2,1)}), bf16[1024,6144]{1,0:T(8,128)(2,1)}) %all-gather.10.cloned.1.call-update) | async-done | bytes 12582928 | tf_op jit(solution)/shard_map/all_gather | solution.py:12
  187.7 0.0 copy-done.12
  187.7 6.2 fusion.10
  193.9 0.0 copy-done.2
  193.9 7.3 multiply_multiply_fusion
  201.2 140.5 %all-gather.12.cloned.1.call-done = bf16[1024,2048]{0,1:T(8,128)(2,1)} async-done(((bf16[1024,64]{0,1:T(8,128)(2,1)}), bf16[1024,2048]{0,1:T(8,128)(2,1)}) %all-gather.12.cloned.1.call-update) | async-done | bytes 4194320 | tf_op jit(solution)/shard_map/all_gather | solution.py:78
  341.7 15.4 %multiply_convert_fusion.1 = bf16[768,2048]{1,0:T(8,128)(2,1)} fusion(bf16[1024,2048]{0,1:T(8,128)(2,1)} %all-gather.12.cloned.1.call-done, f32[2048]{0:T(1024)S(1)} %bitcast.70, f32[768,1024]{1,0:T(8,128)} %multiply_multiply_fusion, bf16[1024,6144]{1,0:T(8,128)(2,1)} %all-gather.10.cloned.1.call-done, f32[1024]{0:T(1024)S(1)} %bitcast.73, ...), kind=kOutput, calls=%fused_computation.13 | convolution fusion | flops 6458179584 | bytes 17861632 | tf_op jit(solution)/shard_map/dot_general | solution.py:76
  357.1 2.3 copy.25
  359.3 26.6 %all_to_all.10 = bf16[2,768,1024]{2,1,0:T(8,128)(2,1)S(1)} all-to-all(bf16[2,768,1024]{2,1,0:T(8,128)(2,1)S(1)} %bitcast.65), channel_id=1, replica_groups=mesh['rep'=2,'fs'=32,'tp'=2] {'tp'}, dimensions={0} | all-to-all | bytes 6291456 | tf_op jit(solution)/shard_map/all_to_all | solution.py:28
  385.9 0.7 convert_reduce_fusion.1
  386.6 0.7 copy-done
  387.3 1.7 fusion.26
  389.0 0.0 all-gather.14.cloned.1.call-update
  389.1 0.0 all-gather.16.cloned.1.call-start
  389.1 0.0 copy-done.5
  389.1 0.7 convert_element_type.94
  389.8 0.0 all-gather.16.cloned.1.call-update
  389.8 0.0 copy-done.7
  389.9 0.0 copy-start.13
  389.9 130.2 %all-gather.20.cloned.1.call-done = bf16[32,44,4096]{2,1,0:T(8,128)(2,1)} async-done(((bf16[1,44,4096]{2,1,0:T(8,128)(2,1)}), bf16[32,44,4096]{2,1,0:T(8,128)(2,1)}) %all-gather.20.cloned.1.call-update) | async-done | bytes 11534352 | tf_op jit(solution)/shard_map/all_gather | solution.py:12
  520.1 14.3 %reshape.44 = bf16[1408,4096]{1,0:T(8,128)(2,1)} reshape(bf16[32,44,4096]{2,1,0:T(8,128)(2,1)} %all-gather.20.cloned.1.call-done) | data formatting | bytes 23068672
  534.4 18.9 %all-gather.14.cloned.1.call-done = bf16[768,2048]{1,0:T(8,128)(2,1)} async-done(((bf16[768,1024]{1,0:T(8,128)(2,1)}), bf16[768,2048]{1,0:T(8,128)(2,1)}) %all-gather.14.cloned.1.call-update) | async-done | bytes 3145744 | tf_op jit(solution)/shard_map/all_gather | solution.py:85
  553.3 2.6 fusion
  555.9 0.0 copy-done.13
  555.9 9.9 %fusion.6 = f32[768,1408]{1,0:T(8,128)} fusion(bf16[1408,4096]{1,0:T(8,128)(2,1)} %reshape.44, bf16[768,2048]{1,0:T(8,128)(2,1)} %all-gather.14.cloned.1.call-done, f32[2048]{0:T(1024)S(1)} %copy-done.13, f32[768]{0:T(1024)S(1)} %add_rsqrt_fusion), kind=kOutput, calls=%fused_computation.14 | convolution fusion | flops 4435476480 | bytes 13249536 | tf_op jit(solution)/shard_map/dot_general | solution.py:91
  565.8 130.3 %all-gather.16.cloned.1.call-done = bf16[1408,2048]{0,1:T(8,128)(2,1)} async-done(((bf16[1408,64]{0,1:T(8,128)(2,1)}), bf16[1408,2048]{0,1:T(8,128)(2,1)}) %all-gather.16.cloned.1.call-update) | async-done | bytes 5767184 | tf_op jit(solution)/shard_map/all_gather | solution.py:97
  696.1 17.4 %multiply_convert_fusion = bf16[768,2048]{1,0:T(8,128)(2,1)} fusion(bf16[1408,2048]{0,1:T(8,128)(2,1)} %all-gather.16.cloned.1.call-done, f32[2048]{0:T(1024)S(1)} %bitcast.69, f32[768,1408]{1,0:T(8,128)} %fusion.6, bf16[1408,4096]{1,0:T(8,128)(2,1)} %reshape.44, f32[1408]{0:T(1024)S(1)} %get-tuple-element.6, f32[1408]{0:T(1024)S(1)} %get-tuple-element.5, ...), kind=kOutput, calls=%fused_computation.11 | convolution fusion | flops 8876457984 | bytes 22181888 | tf_op jit(solution)/shard_map/dot_general | solution.py:95
  713.5 2.3 copy.24
  715.8 26.0 %all_to_all.11 = bf16[2,768,1024]{2,1,0:T(8,128)(2,1)S(1)} all-to-all(bf16[2,768,1024]{2,1,0:T(8,128)(2,1)S(1)} %bitcast.66), channel_id=1, replica_groups=mesh['rep'=2,'fs'=32,'tp'=2] {'tp'}, dimensions={0} | all-to-all | bytes 6291456 | tf_op jit(solution)/shard_map/all_to_all | solution.py:28
  741.8 0.7 convert_reduce_fusion
  742.5 0.7 copy-done.1
  743.2 2.1 fusion.27
  (15 shorter events, 0.2 us)
Async XLA Ops:
  6.5 3.7 copy-start.6
  6.5 4.4 copy-start.4
  6.5 4.5 copy-start.3
  6.5 5.4 copy-start.11
  6.5 5.4 copy-start.10
  6.5 77.8 %copy-start.8 = (f32[3,1024]{1,0:T(4,128)S(1)}, f32[3,1024]{1,0:T(4,128)}, u32[]{:S(2)}) copy-start(f32[3,1024]{1,0:T(4,128)} %param.21) | copy-start | bytes 36868
  6.6 77.9 %copy-start.9 = (f32[3,1024]{1,0:T(4,128)S(1)}, f32[3,1024]{1,0:T(4,128)}, u32[]{:S(2)}) copy-start(f32[3,1024]{1,0:T(4,128)} %param.22) | copy-start | bytes 36868
  6.6 77.9 %all-gather.18.cloned.1.call-start = ((), (), s32[]{:S(2)}) async-start(), calls=%async_computation.6 | async-start | bytes 4718592 | tf_op jit(solution)/shard_map/all_gather | solution.py:56
  7.3 180.4 %all-gather.10.cloned.1.call-start = ((), (), s32[]{:S(2)}) async-start(), calls=%async_computation.2 | async-start | bytes 12976128 | tf_op jit(solution)/shard_map/all_gather | solution.py:12
  10.2 177.5 %copy-start.12 = (f32[2048]{0:T(1024)S(1)}, f32[2048]{0:T(1024)}, u32[]{:S(2)}) copy-start(f32[2048]{0:T(1024)} %param.16) | copy-start | bytes 24580
  10.2 331.5 %all-gather.12.cloned.1.call-start = ((), (), s32[]{:S(2)}) async-start(), calls=%async_computation.3 | async-start | bytes 4325376 | tf_op jit(solution)/shard_map/all_gather | solution.py:78
  10.9 509.2 %all-gather.20.cloned.1.call-start = ((), (), s32[]{:S(2)}) async-start(), calls=%async_computation.7 | async-start | bytes 12976128 | tf_op jit(solution)/shard_map/all_gather | solution.py:12
  11.9 541.5 %all-gather.14.cloned.1.call-start = ((), (), s32[]{:S(2)}) async-start(), calls=%async_computation.4 | async-start | bytes 4718592 | tf_op jit(solution)/shard_map/all_gather | solution.py:85
  87.1 106.8 %copy-start.2 = (bf16[1,768,2048]{2,1,0:T(8,128)(2,1)S(1)}, bf16[1,768,2048]{2,1,0:T(8,128)(2,1)}, u32[]{:S(2)}) copy-start(bf16[1,768,2048]{2,1,0:T(8,128)(2,1)} %all-gather.18.cloned.1.call-done) | copy-start | bytes 9437188
  385.9 1.4 copy-start
  387.3 1.8 copy-start.5
  387.3 2.5 copy-start.7
  389.1 307.1 %all-gather.16.cloned.1.call-start = ((), (), s32[]{:S(2)}) async-start(), calls=%async_computation.5 | async-start | bytes 5947392 | tf_op jit(solution)/shard_map/all_gather | solution.py:97
  389.9 166.0 %copy-start.13 = (f32[2048]{0:T(1024)S(1)}, f32[2048]{0:T(1024)}, u32[]{:S(2)}) copy-start(f32[2048]{0:T(1024)} %param.17) | copy-start | bytes 24580
  741.8 1.4 copy-start.1
Sparse Core Ops, SparseCore 0:
  9.0 18.4 all-gather.17
  29.2 158.4 all-gather.9
  189.3 152.3 all-gather.11
  343.2 176.8 all-gather.19
  521.6 31.6 all-gather.13
  554.8 141.2 all-gather.15
where the time goes:
time: 753 us; the launch traced here: 752 us
  waiting for transfers between devices  521 us (69%)
  blocking collectives  125 us (17%)
  matrix products  56.2 us (7%)
  local copies, waits for them, and re-layouts  20.5 us (3%)
  other arithmetic  15.4 us (2%)
  between operations  13.7 us (2%)
    all_gather x2, waiting for transfers between devices, gather_turned(): out, at, outs = (lax.all_gather(both, axis, axis=0, tiled=True), 0, [])  231 us
    all_gather x1, waiting for transfers between devices, body(): lax.all_gather(mix_out.astype(jnp.bfloat16), 'fs', axis=1, tiled=True)  140 us
    all_gather x1, waiting for transfers between devices, body(): lax.all_gather(ffn_down.astype(jnp.bfloat16), 'fs', axis=1, tiled=True)  130 us
    all_gather x1, blocking collectives, gather_turned(): out, at, outs = (lax.all_gather(both, axis, axis=0, tiled=True), 0, [])  72.3 us
    all_to_all x2, blocking collectives, sent_and_summed(): lax.all_to_all(blocks, axis, split_axis=0, concat_axis=0, tiled=True)  52.5 us
    all_gather x1, waiting for transfers between devices, body(): after_rows = lax.all_gather(after, 'tp', axis=1, tiled=True)  18.9 us
    dot_general x1, matrix products, body(): jnp.dot(hidden, lax.all_gather(ffn_down.astype(jnp.bfloat16), 'fs', axis=...  17.4 us
    unnamed x30, local copies, waits for them, and re-layouts  15.9 us
  transfers between devices with their start and end apart: 6, of which 5 were waited for; matrix products, arithmetic and copies ran while one was open for 9% of the time, Pallas kernels for 0%

commit v1 on v0

--- a/solution.py
+++ b/solution.py
@@ -75,7 +75,12 @@
     mixer_terms = (
         jnp.dot(
             gated,
-            lax.all_gather(mix_out.astype(jnp.bfloat16), "fs", axis=1, tiled=True),
+            jnp.concatenate(
+                lax.all_to_all(
+                    jnp.stack([mix_out.astype(jnp.bfloat16)] * lax.axis_size("fs")), "fs", 0, 0
+                ),
+                axis=1,
+            ),
             preferred_element_type=jnp.float32,
         )
         * scale

time: 753 us -> 624 us (0.83)
  waiting for transfers between devices: 521 us -> 327 us
  blocking collectives: 125 us -> 180 us
  starting transfers between devices: 0.24 us -> 9.65 us
    all_gather x1 -> x0, waiting for transfers between devices: 140 us -> none  [body(): lax.all_gather(mix_out.astype(jnp.bfloat16), 'fs', axis=1, tiled=True)]
    all_gather x1, blocking collectives: 72.3 us -> 131 us  [gather_turned(): out, at, outs = (lax.all_gather(both, axis, axis=0, tiled=True), 0, [])]
    all_gather x2, waiting for transfers between devices: 231 us -> 177 us  [gather_turned(): out, at, outs = (lax.all_gather(both, axis, axis=0, tiled=True), 0, [])]
    all_to_all x0 -> x1, starting transfers between devices: none -> 9.49 us  [body(): lax.all_to_all(jnp.stack([mix_out.astype(jnp.bfloat16)] * lax.axis_size('...]
  transfers between devices with their start and end apart: 6 -> 6, of which waited for: 5 -> 4; matrix products, arithmetic and copies ran while one was open for 9% -> 11% of each run, Pallas kernels for 0% -> 0%
where the time goes in v1:
time: 624 us; the launch traced here: 623 us
  waiting for transfers between devices  327 us (52%)
  blocking collectives  180 us (29%)
  matrix products  56.1 us (9%)
  local copies, waits for them, and re-layouts  22.9 us (4%)
  other arithmetic  14.7 us (2%)
  between operations  13.4 us (2%)
  starting transfers between devices  9.65 us (2%)
    all_gather x2, waiting for transfers between devices, gather_turned(): out, at, outs = (lax.all_gather(both, axis, axis=0, tiled=True), 0, [])  177 us
    all_gather x1, blocking collectives, gather_turned(): out, at, outs = (lax.all_gather(both, axis, axis=0, tiled=True), 0, [])  131 us
    all_gather x1, waiting for transfers between devices, body(): lax.all_gather(ffn_down.astype(jnp.bfloat16), 'fs', axis=1, tiled=True)  130 us
    all_to_all x2, blocking collectives, sent_and_summed(): lax.all_to_all(blocks, axis, split_axis=0, concat_axis=0, tiled=True)  48.5 us
    all_gather x1, waiting for transfers between devices, body(): after_rows = lax.all_gather(after, 'tp', axis=1, tiled=True)  19 us
    dot_general x1, matrix products, body(): jnp.dot(hidden, lax.all_gather(ffn_down.astype(jnp.bfloat16), 'fs', axis=...  17.4 us
    unnamed x30, local copies, waits for them, and re-layouts  15.9 us
    dot_general x1, matrix products, body(): jnp.dot(gated, jnp.concatenate(lax.all_to_all(jnp.stack([mix_out.astype(j...  15.2 us
  transfers between devices with their start and end apart: 6, of which 4 were waited for; matrix products, arithmetic and copies ran while one was open for 11% of the time, Pallas kernels for 0%

profile of v1, /device:TPU:1, one launch (start us, length us, event | category | flops | bytes accessed | tf_op | source)
XLA Modules:
  0.0 623.4 jit_solution(616493204678986122)
XLA Ops:
  6.5 0.0 copy-start.4
  6.5 0.0 copy-start.3
  6.5 0.0 copy-start.6
  6.5 0.0 all-gather.15.cloned.1.call-start
  6.5 0.7 all-gather.15.cloned.1.call-update
  7.3 0.0 all-gather.9.cloned.1.call-start
  7.3 1.0 convert_bitcast_fusion.5
  8.3 1.1 convert_bitcast_fusion.3
  9.3 0.8 pad_maximum_fusion
  10.1 0.0 all-gather.9.cloned.1.call-update
  10.1 0.0 all-gather.17.cloned.1.call-start
  10.2 0.0 copy-done.4
  10.2 0.0 copy-done.3
  10.3 0.8 maximum_bitcast_fusion
  11.1 0.0 all-gather.17.cloned.1.call-update
  11.1 0.0 copy-done.6
  11.1 2.5 stack.2
  13.6 0.0 copy-start.10
  13.6 0.0 copy-start.11
  13.6 0.0 copy-start.8
  13.6 9.5 %all-to-all-start = ((bf16[32,1024,64]{1,2,0:T(8,128)(2,1)}), bf16[32,1024,64]{1,2,0:T(8,128)(2,1)}, u32[]{:S(2)}, u32[]{:S(2)}) async-start(bf16[32,1024,64]{1,2,0:T(8,128)(2,1)} %stack.2), calls=%async_computation | async-start | bytes 8388608 | tf_op jit(solution)/shard_map/all_to_all | solution.py:79
  23.1 0.0 copy-start.12
  23.1 0.0 all-gather.11.cloned.1.call-start
  23.2 0.0 copy-done.10
  23.2 0.0 copy-done.11
  23.2 131.0 %all-gather.1 = f32[32,64,2]{1,2,0:T(2,128)S(1)} all-gather(f32[1,64,2]{1,2,0:T(2,128)S(1)} %maximum_bitcast_fusion.1), channel_id=1, replica_groups=mesh['rep'=2,'fs'=32,'tp'=2] {'fs'}, dimensions={0}, use_global_device_ids=true | all-gather | bytes 16896 | tf_op jit(solution)/shard_map/all_gather | solution.py:12
  154.2 0.1 reshape.52
  154.3 0.0 copy-done.8
  154.4 0.0 copy-done.9
  154.4 0.0 all-gather.15.cloned.1.call-done
  154.4 2.6 fusion.3
  157.0 0.0 copy-start.2
  157.1 61.3 %all-gather.9.cloned.1.call-done = bf16[1024,6144]{1,0:T(8,128)(2,1)} async-done(((bf16[32,6144]{1,0:T(8,128)(2,1)}), bf16[1024,6144]{1,0:T(8,128)(2,1)}) %all-gather.9.cloned.1.call-update) | async-done | bytes 12582928 | tf_op jit(solution)/shard_map/all_gather | solution.py:12
  218.4 0.0 copy-done.12
  218.4 6.2 fusion.10
  224.6 0.0 copy-done.2
  224.6 7.3 %multiply_multiply_fusion = f32[768,1024]{1,0:T(8,128)} fusion(f32[768,1024]{1,0:T(8,128)S(1)} %fusion.10, bf16[1024,6144]{1,0:T(8,128)(2,1)} %all-gather.9.cloned.1.call-done, f32[1024]{0:T(1024)S(1)} %bitcast.78, f32[1024]{0:T(1024)S(1)} %bitcast.79, bf16[1,768,2048]{2,1,0:T(8,128)(2,1)S(1)} %copy-done.2, f32[2048]{0:T(1024)S(1)} %copy-done.12, ...), kind=kOutput, calls=%fused_computation.42 | convolution fusion | flops 3229876224 | bytes 13650944 | tf_op jit(solution)/shard_map/dot_general | solution.py:66
  231.9 0.0 all-to-all-done
  231.9 15.2 %multiply_convert_fusion.1 = bf16[768,2048]{1,0:T(8,128)(2,1)} fusion(bf16[1024,2048]{0,1:T(8,128)(2,1)} %bitcast.12, f32[2048]{0:T(1024)S(1)} %bitcast.73, f32[768,1024]{1,0:T(8,128)} %multiply_multiply_fusion, bf16[1024,6144]{1,0:T(8,128)(2,1)} %all-gather.9.cloned.1.call-done, f32[1024]{0:T(1024)S(1)} %bitcast.76, f32[1024]{0:T(1024)S(1)} %bitcast.77, ...), kind=kOutput, calls=%fused_computation.13 | convolution fusion | flops 6458179584 | bytes 17861632 | tf_op jit(solution)/shard_map/dot_general | solution.py:76
  247.2 2.3 copy.26
  249.4 22.6 %all_to_all.15 = bf16[2,768,1024]{2,1,0:T(8,128)(2,1)S(1)} all-to-all(bf16[2,768,1024]{2,1,0:T(8,128)(2,1)S(1)} %bitcast.68), channel_id=1, replica_groups=mesh['rep'=2,'fs'=32,'tp'=2] {'tp'}, dimensions={0} | all-to-all | bytes 6291456 | tf_op jit(solution)/shard_map/all_to_all | solution.py:28
  272.0 0.7 convert_reduce_fusion.1
  272.7 0.7 copy-done
  273.4 1.7 fusion.26
  275.1 0.0 all-gather.11.cloned.1.call-update
  275.2 0.0 all-gather.13.cloned.1.call-start
  275.2 0.0 copy-done.5
  275.2 0.7 convert_element_type.94
  275.9 0.0 all-gather.13.cloned.1.call-update
  275.9 0.0 copy-done.7
  276.0 0.0 copy-start.13
  276.0 115.6 %all-gather.17.cloned.1.call-done = bf16[32,44,4096]{2,1,0:T(8,128)(2,1)} async-done(((bf16[1,44,4096]{2,1,0:T(8,128)(2,1)}), bf16[32,44,4096]{2,1,0:T(8,128)(2,1)}) %all-gather.17.cloned.1.call-update) | async-done | bytes 11534352 | tf_op jit(solution)/shard_map/all_gather | solution.py:12
  391.6 14.3 %reshape.54 = bf16[1408,4096]{1,0:T(8,128)(2,1)} reshape(bf16[32,44,4096]{2,1,0:T(8,128)(2,1)} %all-gather.17.cloned.1.call-done) | data formatting | bytes 23068672
  405.9 19.0 %all-gather.11.cloned.1.call-done = bf16[768,2048]{1,0:T(8,128)(2,1)} async-done(((bf16[768,1024]{1,0:T(8,128)(2,1)}), bf16[768,2048]{1,0:T(8,128)(2,1)}) %all-gather.11.cloned.1.call-update) | async-done | bytes 3145744 | tf_op jit(solution)/shard_map/all_gather | solution.py:90
  425.0 2.6 fusion
  427.5 0.0 copy-done.13
  427.5 9.9 %fusion.6 = f32[768,1408]{1,0:T(8,128)} fusion(bf16[1408,4096]{1,0:T(8,128)(2,1)} %reshape.54, bf16[768,2048]{1,0:T(8,128)(2,1)} %all-gather.11.cloned.1.call-done, f32[2048]{0:T(1024)S(1)} %copy-done.13, f32[768]{0:T(1024)S(1)} %add_rsqrt_fusion), kind=kOutput, calls=%fused_computation.14 | convolution fusion | flops 4435476480 | bytes 13249536 | tf_op jit(solution)/shard_map/dot_general | solution.py:96
  437.4 130.3 %all-gather.13.cloned.1.call-done = bf16[1408,2048]{0,1:T(8,128)(2,1)} async-done(((bf16[1408,64]{0,1:T(8,128)(2,1)}), bf16[1408,2048]{0,1:T(8,128)(2,1)}) %all-gather.13.cloned.1.call-update) | async-done | bytes 5767184 | tf_op jit(solution)/shard_map/all_gather | solution.py:102
  567.7 17.4 %multiply_convert_fusion = bf16[768,2048]{1,0:T(8,128)(2,1)} fusion(bf16[1408,2048]{0,1:T(8,128)(2,1)} %all-gather.13.cloned.1.call-done, f32[2048]{0:T(1024)S(1)} %bitcast.72, f32[768,1408]{1,0:T(8,128)} %fusion.6, bf16[1408,4096]{1,0:T(8,128)(2,1)} %reshape.54, f32[1408]{0:T(1024)S(1)} %get-tuple-element.6, f32[1408]{0:T(1024)S(1)} %get-tuple-element.5, ...), kind=kOutput, calls=%fused_computation.11 | convolution fusion | flops 8876457984 | bytes 22181888 | tf_op jit(solution)/shard_map/dot_general | solution.py:100
  585.1 2.3 copy.25
  587.4 26.0 %all_to_all.16 = bf16[2,768,1024]{2,1,0:T(8,128)(2,1)S(1)} all-to-all(bf16[2,768,1024]{2,1,0:T(8,128)(2,1)S(1)} %bitcast.69), channel_id=1, replica_groups=mesh['rep'=2,'fs'=32,'tp'=2] {'tp'}, dimensions={0} | all-to-all | bytes 6291456 | tf_op jit(solution)/shard_map/all_to_all | solution.py:28
  613.4 0.7 convert_reduce_fusion
  614.1 0.7 copy-done.1
  614.8 2.1 fusion.27
  (15 shorter events, 0.2 us)
Async XLA Ops:
  6.5 3.7 copy-start.4
  6.5 3.7 copy-start.3
  6.5 4.6 copy-start.6
  6.5 147.9 %all-gather.15.cloned.1.call-start = ((), (), s32[]{:S(2)}) async-start(), calls=%async_computation.6 | async-start | bytes 4718592 | tf_op jit(solution)/shard_map/all_gather | solution.py:56
  7.3 211.1 %all-gather.9.cloned.1.call-start = ((), (), s32[]{:S(2)}) async-start(), calls=%async_computation.3 | async-start | bytes 12976128 | tf_op jit(solution)/shard_map/all_gather | solution.py:12
  10.1 381.5 %all-gather.17.cloned.1.call-start = ((), (), s32[]{:S(2)}) async-start(), calls=%async_computation.7 | async-start | bytes 12976128 | tf_op jit(solution)/shard_map/all_gather | solution.py:12
  13.6 9.6 %copy-start.10 = (f32[64]{0:T(128)S(1)}, f32[64]{0:T(128)}, u32[]{:S(2)}) copy-start(f32[64]{0:T(128)} %param.29) | copy-start | bytes 772
  13.6 9.6 %copy-start.11 = (f32[64]{0:T(128)S(1)}, f32[64]{0:T(128)}, u32[]{:S(2)}) copy-start(f32[64]{0:T(128)} %param.24) | copy-start | bytes 772
  13.6 140.7 %copy-start.8 = (f32[3,1024]{1,0:T(4,128)S(1)}, f32[3,1024]{1,0:T(4,128)}, u32[]{:S(2)}) copy-start(f32[3,1024]{1,0:T(4,128)} %param.21) | copy-start | bytes 36868
  13.6 140.7 %copy-start.9 = (f32[3,1024]{1,0:T(4,128)S(1)}, f32[3,1024]{1,0:T(4,128)}, u32[]{:S(2)}) copy-start(f32[3,1024]{1,0:T(4,128)} %param.22) | copy-start | bytes 36868
  13.6 218.3 %all-to-all-start = ((bf16[32,1024,64]{1,2,0:T(8,128)(2,1)}), bf16[32,1024,64]{1,2,0:T(8,128)(2,1)}, u32[]{:S(2)}, u32[]{:S(2)}) async-start(bf16[32,1024,64]{1,2,0:T(8,128)(2,1)} %stack.2), calls=%async_computation | async-start | bytes 8388608 | tf_op jit(solution)/shard_map/all_to_all | solution.py:79
  23.1 195.3 %copy-start.12 = (f32[2048]{0:T(1024)S(1)}, f32[2048]{0:T(1024)}, u32[]{:S(2)}) copy-start(f32[2048]{0:T(1024)} %param.16) | copy-start | bytes 24580
  23.1 401.8 %all-gather.11.cloned.1.call-start = ((), (), s32[]{:S(2)}) async-start(), calls=%async_computation.4 | async-start | bytes 4718592 | tf_op jit(solution)/shard_map/all_gather | solution.py:90
  157.0 67.6 %copy-start.2 = (bf16[1,768,2048]{2,1,0:T(8,128)(2,1)S(1)}, bf16[1,768,2048]{2,1,0:T(8,128)(2,1)}, u32[]{:S(2)}) copy-start(bf16[1,768,2048]{2,1,0:T(8,128)(2,1)} %all-gather.15.cloned.1.call-done) | copy-start | bytes 9437188
  272.0 1.4 copy-start
  273.4 1.8 copy-start.5
  273.4 2.5 copy-start.7
  275.2 292.6 %all-gather.13.cloned.1.call-start = ((), (), s32[]{:S(2)}) async-start(), calls=%async_computation.5 | async-start | bytes 5947392 | tf_op jit(solution)/shard_map/all_gather | solution.py:102
  276.0 151.5 %copy-start.13 = (f32[2048]{0:T(1024)S(1)}, f32[2048]{0:T(1024)}, u32[]{:S(2)}) copy-start(f32[2048]{0:T(1024)} %param.17) | copy-start | bytes 24580
  613.4 1.4 copy-start.1
Sparse Core Ops, SparseCore 0:
  9.0 18.4 all-gather.14
  29.1 189.2 all-gather.8
  220.0 171.5 all-gather.16
  393.1 31.7 all-gather.10
  426.4 141.2 all-gather.12
